TPU v7x, 256 devices: a 8x8x2 block of a 8x8x16 slice. The times are simulated.
256 devices in a mesh: grp: 2 (over z), sp: 16 (over y, core), tp: 8 (over x).
Axes of the slice: x: 8, y: 8, z: 2, core: 2. Of those that a mesh axis runs over, the one named last changes fastest.
The devices are a block of a 8x8x16 slice.
Arguments:
- residual: bfloat16 [32768, 2048], P(('grp', 'sp', 'tp')), parts along dimension 0, may hold values from -6 to 6
- grouped_value_heads: bfloat16 [32768, 2, 1024], P(('grp', 'sp'), None, 'tp'), parts along dimension 0, may hold values from -6 to 6
- output_gate_heads: bfloat16 [32768, 2, 1024], P(('grp', 'sp'), None, 'tp'), parts along dimension 0, may hold values from -6 to 6
- projected_key_query: bfloat16 [32768, 384], P(('grp', 'sp')), parts along dimension 0, may hold values from -6 to 6
- raw_step_size: bfloat16 [32768, 2, 16], P(('grp', 'sp'), None, 'tp'), parts along dimension 0, may hold values from -3 to 3
- step_size_bias: float32 [2, 16], P(None, 'tp'), may hold values from -1 to 0.5
- head_decay_logarithm: float32 [2, 16], P(None, 'tp'), may hold values from -16 to -2
- position_extra_decay: float32 [32768], P(('grp', 'sp')), parts along dimension 0, may hold values from -0.7 to 0
- head_skip_weight: float32 [2, 16], P(None, 'tp'), may hold values from 0.5 to 2
- value_kernel_taps: bfloat16 [4, 2, 1024], P(None, None, 'tp'), may hold values from -3 to 3
- key_query_kernel: bfloat16 [4, 384], replicated, may hold values from -3 to 3
- head_norm_gain: float32 [2, 1024], P(None, 'tp'), may hold values from 0.1 to 1.9
- output_matrix: bfloat16 [2, 1024, 2048], P(None, 'tp'), may hold values from -0.125 to 0.125
- expert_norm_gain: float32 [2048], replicated, may hold values from 0.1 to 1.9
- expert_gate_weight: bfloat16 [16, 2048, 4096], P('sp', None, 'tp'), may hold values from -0.125 to 0.125
- expert_up_weight: bfloat16 [16, 2048, 4096], P('sp', None, 'tp'), may hold values from -0.125 to 0.125
- expert_down_weight: bfloat16 [16, 4096, 2048], P('sp', 'tp'), may hold values from -0.09375 to 0.09375
- token_expert_choice: int32 [32768, 2], P(('grp', 'sp', 'tp')), parts along dimension 0, may hold values from 0 to 15, all different within a row; in each aligned block of 128 rows (0 to 127, 128 to 255, ...) at most 17 rows name the same one
- expert_output_weight: float32 [32768, 2], P(('grp', 'sp', 'tp')), parts along dimension 0, may hold values from 0.2 to 1
Outputs:
- layer_out: bfloat16 [32768, 2048], P(('grp', 'sp', 'tp')), parts along dimension 0
There are 2 independent parts, one for each index of `grp`. A program takes and returns all parts, laid end to end along the dimension named above; an argument that names none is the same for every part. Nothing has to cross between parts.
Inputs may be any that keep to these rules, and one draw needn't show every extreme that they name: `token_expert_choice`: each row names two different experts. The token rows of one device name one expert at most 17 times.
All inputs are finite; a program needn't handle non-finite values.
Results may differ from a plain program's by a relative error of at most 0.015.
Values may be sent and summed in bfloat16 or wider, within the bound.
A program may use at most 128 MiB of HBM per device.

v0:
```python
import functools

import jax
import jax.numpy as jnp
from jax import lax
from jax.experimental import pallas as pl
from jax.experimental.pallas import tpu as pltpu
from jax.sharding import PartitionSpec as P

HEAD_DIM = 64
STATE_ONE = 64
STATE_TWO = 128
BLOCK = 128


EPSILON = 1e-06


def passed_along(shard, axis, by):
    length = lax.axis_size(axis)
    pairs = [(i, i + by) for i in range(length) if 0 <= i + by < length]
    return lax.ppermute(shard, axis, pairs)


def sent_to_all(shard, axis):
    length = lax.axis_size(axis)
    return lax.all_to_all(
        jnp.broadcast_to(shard[None], (length, *shard.shape)), axis, 0, 0, tiled=True
    )


def all_in_one(shard, axis):
    leaves = jax.tree.leaves(shard)
    turns = sorted(range(len(leaves)), key=lambda k: -leaves[k].size)
    width = (1, *leaves[turns[0]].shape)[-1]
    lines = [
        jnp.pad(leaves[k].reshape(-1), (0, -leaves[k].size % width)).reshape(-1, width)
        for k in turns
    ]
    both, at, found = (sent_to_all(jnp.concatenate(lines), axis), 0, {})
    for k, line in zip(turns, lines):
        section = both[:, at : at + len(line)].reshape(len(both), -1)
        found[k] = section[:, : leaves[k].size].reshape(-1, *leaves[k].shape)
        at += len(line)
    numbers = iter(range(len(leaves)))
    return jax.tree.map(lambda _: found[next(numbers)], shard)


def joined_by_halves(pieces, combine):
    while len(jax.tree.leaves(pieces)[0]) > 1:
        pieces = jax.vmap(combine)(
            *(jax.tree.map(lambda part: part[side::2], pieces) for side in (0, 1))
        )
    return jax.tree.map(lambda part: part[0], pieces)


def entering_2(shard, axis, combine, identity):
    length, place = (lax.axis_size(axis), lax.axis_index(axis))
    passed = jnp.arange(length) < place

    def kept(part, zero, own):
        part = jnp.where(
            passed.reshape(-1, *(1 for _ in own.shape)),
            part.astype(own.dtype),
            jnp.asarray(zero, own.dtype),
        )
        return part

    pieces = all_in_one(
        jax.tree.map(
            lambda part, kind: part.astype(kind), shard, (jnp.bfloat16, jnp.bfloat16, jnp.bfloat16)
        ),
        axis,
    )
    return joined_by_halves(jax.tree.map(kept, pieces, identity, shard), combine)


def causal_taps(extended, tap_weights, length):
    summed = jnp.zeros((length, extended.shape[1]), jnp.float32)
    for offset in range(tap_weights.shape[0]):
        summed = summed + extended[offset : offset + length].astype(jnp.float32) * tap_weights[
            offset
        ].astype(jnp.float32)
    return summed


def advance(carried, pair_item):
    block_state, fading_step = pair_item
    return (carried * fading_step[:, None, None] + block_state, carried)


def local_blocks(value_rows, key_rows, query_rows, step_spacing, decay_logarithm):
    positions, head_count, head_width = value_rows.shape
    block_count = positions // BLOCK
    value_rows = value_rows.reshape(block_count, BLOCK, head_count, head_width)
    key_rows = key_rows.reshape(block_count, BLOCK, key_rows.shape[-1])
    query_rows = query_rows.reshape(block_count, BLOCK, query_rows.shape[-1])
    step_spacing = step_spacing.reshape(block_count, BLOCK, head_count)
    running = jnp.cumsum(decay_logarithm.reshape(block_count, BLOCK, head_count), axis=1)
    scores = jnp.einsum("kln,ksn->kls", query_rows, key_rows, preferred_element_type=jnp.float32)
    causal = jnp.tril(jnp.ones((BLOCK, BLOCK), jnp.bool_))
    spread = running[:, :, None, :] - running[:, None, :, :]
    damping = jnp.exp(jnp.where(causal[None, :, :, None], spread, -jnp.inf))
    weights = (scores[:, :, :, None] * damping * step_spacing[:, None, :, :]).astype(jnp.bfloat16)
    near_part = jnp.einsum(
        "klsh,kshp->klhp", weights, value_rows, preferred_element_type=jnp.float32
    )
    fading = jnp.exp(running[:, -1:, :] - running) * step_spacing
    scaled_keys = (key_rows.astype(jnp.float32)[:, :, None, :] * fading[:, :, :, None]).astype(
        jnp.bfloat16
    )
    states = jnp.einsum(
        "kshn,kshp->khpn", scaled_keys, value_rows, preferred_element_type=jnp.float32
    )
    block_ends = running[:, -1, :]
    anchor = jnp.zeros(states.shape[1:], jnp.float32)
    last_state, entering = lax.scan(advance, anchor, (states, jnp.exp(block_ends)))
    wide_queries = query_rows.astype(jnp.float32)
    far_part = jnp.einsum("kln,khpn->klhp", wide_queries, entering, precision=lax.Precision.HIGHEST)
    far_part = far_part * jnp.exp(running)[:, :, :, None]
    earlier_ends = jnp.cumsum(block_ends, axis=0) - block_ends
    carried_decay = jnp.exp(running + earlier_ends[:, None, :])
    return (
        near_part + far_part,
        last_state,
        jnp.sum(block_ends, axis=0),
        wide_queries,
        carried_decay,
    )


def join_states(earlier, later):
    early_decay, early_one, early_two = earlier
    late_decay, late_one, late_two = later
    return (
        early_decay + late_decay,
        early_one * jnp.exp(late_decay[0])[:, None, None] + late_one,
        early_two * jnp.exp(late_decay[1])[:, None, None] + late_two,
    )


MESH = pl.DeviceIdType.MESH
PIECE = 256
VMEM_LIMIT = 67043328


def expert_kernel(
    dims,
    stream_ref,
    gain_ref,
    choice_ref,
    share_ref,
    gate_hbm,
    up_hbm,
    down_hbm,
    out_ref,
    table,
    outbound,
    over_out,
    over_in,
    chunks,
    hidden,
    gate_up,
    down,
    sum_right,
    sum_left,
    totals,
    over_total,
    over_back,
    returned,
    over_ret,
    pick,
    load_sem,
    out_send,
    out_recv,
    over_send,
    over_recv,
    ring_send,
    ring_recv,
    sum_send,
    sum_recv,
    back_send,
    back_recv,
):
    f32, bf16 = jnp.float32, jnp.bfloat16
    places, columns, rows, main, over = dims["S"], dims["X"], dims["R"], dims["M"], dims["OV"]
    pieces, tiles, slots = dims["NP"], dims["NT"], dims["S"] * dims["M"]
    half = columns // 2
    me_x, me_s = lax.axis_index("tp"), lax.axis_index("sp")
    right = {"tp": lax.rem(me_x + 1, columns)}
    left = {"tp": lax.rem(me_x + columns - 1, columns)}

    def column(offset):
        return lax.rem(me_x + offset + columns, columns)

    def place(offset):
        return lax.rem(me_s + offset, places)

    def lines(index):
        return pl.ds(pl.multiple_of(index * main, main), main)

    def remote(src, dst, send, recv, device):
        return pltpu.make_async_remote_copy(
            src_ref=src, dst_ref=dst, send_sem=send, recv_sem=recv, device_id=device, device_id_type=MESH
        )

    loads = []
    for t in range(tiles):
        span = pl.ds(t * 128, 128)
        loads.append((gate_hbm.at[0, :, span], gate_up.at[t, :, pl.ds(0, 128)]))
        loads.append((up_hbm.at[0, :, span], gate_up.at[t, :, pl.ds(128, 128)]))
    for p in range(pieces):
        loads.append((down_hbm.at[0, :, pl.ds(p * PIECE, PIECE)], down.at[p]))
    loads = [pltpu.make_async_copy(a, b, load_sem.at[n]) for n, (a, b) in enumerate(loads)]
    for load in loads:
        load.start()

    barrier = pltpu.get_barrier_semaphore()
    for neighbour in (left, right):
        pl.semaphore_signal(barrier, inc=1, device_id=neighbour, device_id_type=MESH)
    for i in range(1, places):
        pl.semaphore_signal(barrier, inc=1, device_id={"sp": place(i)}, device_id_type=MESH)

    expert_at = lax.broadcasted_iota(jnp.int32, (over, rows), 0)
    token_a = lax.broadcasted_iota(jnp.int32, (rows, rows), 0)
    token_b = lax.broadcasted_iota(jnp.int32, (rows, rows), 1)
    choice = choice_ref[...]
    named = jnp.where((expert_at == choice[0:1]) | (expert_at == choice[1:2]), 1.0, 0.0)
    rank = jnp.dot(
        named.astype(bf16), jnp.where(token_a < token_b, 1.0, 0.0).astype(bf16), preferred_element_type=f32
    )
    slot_row = lax.broadcasted_iota(jnp.int32, (slots, over), 0)
    slot_expert = lax.broadcasted_iota(jnp.int32, (slots, over), 1) * main
    spread = jnp.where((slot_row >= slot_expert) & (slot_row < slot_expert + main), 1.0, 0.0).astype(bf16)
    named_x = jnp.dot(spread, named.astype(bf16), preferred_element_type=f32)
    rank_x = jnp.dot(spread, rank.astype(bf16), preferred_element_type=f32)
    turn = jnp.bitwise_and(lax.broadcasted_iota(jnp.int32, (slots, rows), 0), main - 1).astype(f32)
    put_main = jnp.where(rank_x == turn, named_x, 0.0).astype(bf16)
    put_over = jnp.where(rank == float(main), named, 0.0).astype(bf16)

    wide = stream_ref[...].astype(f32)
    scale = lax.rsqrt(jnp.mean(wide * wide, axis=1, keepdims=True) + EPSILON)
    normed = (wide * scale * gain_ref[...]).astype(bf16)
    for p in range(pieces):
        part = normed[:, p * PIECE : (p + 1) * PIECE]
        outbound[p] = jnp.dot(put_main, part, preferred_element_type=f32).astype(bf16)
        spill = jnp.dot(put_over, part, preferred_element_type=f32)
        for c in range(PIECE // 128):
            over_out[:, p * (PIECE // 128) + c, :] = spill[:, c * 128 : (c + 1) * 128]

    pl.semaphore_wait(barrier, 2 + places - 1)

    for i in range(1, places):
        remote(
            over_out.at[place(i)], over_in.at[me_s], over_send.at[0], over_recv.at[0], {"sp": place(i)}
        ).start()

    def send_out(p, carry):
        for i in range(1, places):
            remote(
                outbound.at[p, lines(place(i)), :],
                chunks.at[me_x, p, lines(me_s), :],
                out_send.at[p],
                out_recv.at[p],
                {"sp": place(i)},
            ).start()
        chunks[me_x, p, lines(me_s), :] = outbound[p, lines(me_s), :]
        return carry

    lax.fori_loop(0, pieces, send_out, 0)
    over_in[me_s] = over_out[me_s]
    if places < over:
        over_in[places:over] = jnp.zeros((over - places, *over_in.shape[1:]), f32)
        over_ret[places:over] = jnp.zeros((over - places, *over_ret.shape[1:]), f32)

    table[...] = jnp.zeros_like(table)
    table[0:2] = choice.astype(f32)
    table[2:4] = share_ref[...]
    turned = jnp.transpose(table[...])
    expert_to = lax.broadcasted_iota(jnp.int32, (rows, over), 1).astype(f32)
    named_k = [jnp.where(expert_to == turned[:, k : k + 1], 1.0, 0.0) for k in range(2)]
    rank_t = jnp.dot(
        jnp.where(token_b < token_a, 1.0, 0.0).astype(bf16),
        (named_k[0] + named_k[1]).astype(bf16),
        preferred_element_type=f32,
    )
    total_slots = slots + over
    slot_col = lax.broadcasted_iota(jnp.int32, (over, total_slots), 1)
    slot_exp = lax.broadcasted_iota(jnp.int32, (over, total_slots), 0)
    low = slot_exp * main
    spread_t = jnp.where(
        ((slot_col < slots) & (slot_col >= low) & (slot_col < low + main)) | (slot_col == slots + slot_exp), 1.0, 0.0
    ).astype(bf16)
    at = lax.broadcasted_iota(jnp.int32, (rows, total_slots), 1)
    turn_t = jnp.where(at < slots, jnp.bitwise_and(at, main - 1), main).astype(f32)
    rank_tx = jnp.dot(rank_t.astype(bf16), spread_t, preferred_element_type=f32)
    for k in range(2):
        named_tx = jnp.dot(named_k[k].astype(bf16), spread_t, preferred_element_type=f32)
        pick[k] = jnp.where(rank_tx == turn_t, named_tx, 0.0).astype(bf16)

    remote(
        over_out.at[0 : places - 1], over_in.at[0 : places - 1], over_send.at[0], over_recv.at[0], right
    ).wait_recv()
    for c in range(dims["NC"]):
        at_piece, at_lane = c // (PIECE // 128), (c % (PIECE // 128)) * 128
        chunks[me_x, at_piece, slots : slots + over, at_lane : at_lane + 128] = over_in[:, c, :].astype(bf16)

    def ring(way, step, p, col):
        return remote(
            chunks.at[col, p],
            chunks.at[col, p],
            ring_send.at[way, step, p],
            ring_recv.at[way, step, p],
            right if way == 0 else left,
        )

    def far(way, p):
        odd = lax.rem(p, 2)
        return half - odd if way == 0 else half - 1 + odd

    def unit(col, t):
        acc = jnp.dot(chunks[col, 0], gate_up[t, 0:PIECE, :], preferred_element_type=f32)
        for q in range(1, pieces):
            acc = acc + jnp.dot(
                chunks[col, q], gate_up[t, q * PIECE : (q + 1) * PIECE, :], preferred_element_type=f32
            )
        gate, up = acc[:, 0:128], acc[:, 128:256]
        value = gate * (1.0 / (1.0 + jnp.exp(-gate))) * up
        hidden[col, :, pl.ds(pl.multiple_of(t * 128, 128), 128)] = value.astype(bf16)

    def start_piece(p, carry):
        remote(
            outbound.at[p, 0 : (places - 1) * main, :],
            chunks.at[me_x, p, 0 : (places - 1) * main, :],
            out_send.at[p],
            out_recv.at[p],
            right,
        ).wait_recv()
        ring(0, 0, p, me_x).start()
        ring(1, 0, p, me_x).start()
        return carry

    lax.fori_loop(0, pieces, start_piece, 0)
    for load in loads:
        load.wait()

    for k in range(1, half + 1):

        def pass_on(p, carry, k=k):
            for way in range(2):
                col = column(-k if way == 0 else k)

                @pl.when(k <= far(way, p))
                def _():
                    ring(way, k - 1, p, col).wait_recv()

                if k < half:

                    @pl.when(k < far(way, p))
                    def _():
                        ring(way, k, p, col).start()

            if k == 1:

                @pl.when(lax.rem(p, 2) == 0)
                def _():
                    unit(me_x, lax.div(p, 2))

            else:
                side = lax.div(p, tiles)
                unit(column((2 * side - 1) * (k - 1)), lax.rem(p, tiles))
            return carry

        lax.fori_loop(0, pieces, pass_on, 0)

    def last_unit(t, carry):
        unit(column(half), t)
        return carry

    lax.fori_loop(0, tiles, last_unit, 0)

    def own(col, p):
        return jnp.dot(hidden[col], down[p], preferred_element_type=f32)

    def hop(way, j, p):
        buffer = sum_right if way == 0 else sum_left
        return remote(
            buffer.at[j, p],
            buffer.at[j - 1, p],
            sum_send.at[way, j - 1, p],
            sum_recv.at[way, j - 1, p],
            right if way == 0 else left,
        )

    def round_of(t, low_piece, high_piece):
        def body(p, carry):
            for way in range(2):
                buffer = sum_right if way == 0 else sum_left
                j = far(1 - way, p) - t

                def work(way=way, buffer=buffer, j=j):
                    value = own(column(j if way == 0 else -j), p)
                    if t > 0:
                        hop(way, j + 1, p).wait_recv()
                        value = value + buffer[j, p].astype(f32)
                    buffer[j, p] = value.astype(bf16)
                    hop(way, j, p).start()

                if t < half - 1:
                    work()
                else:
                    pl.when(j >= 1)(work)
            return carry

        lax.fori_loop(low_piece, high_piece, body, 0)

    def finish(low_piece, high_piece):
        def body(p, carry):
            value = own(me_x, p)
            hop(0, 1, p).wait_recv()
            hop(1, 1, p).wait_recv()
            value = value + sum_right[0, p].astype(f32) + sum_left[0, p].astype(f32)
            totals[p] = value[0:slots].astype(bf16)
            over_total[p] = value[slots : slots + over]
            returned[p, lines(me_s), :] = totals[p, lines(me_s), :]
            for i in range(1, places):
                remote(
                    totals.at[p, lines(place(i)), :],
                    returned.at[p, lines(me_s), :],
                    back_send.at[p],
                    back_recv.at[p],
                    {"sp": place(i)},
                ).start()
            return carry

        lax.fori_loop(low_piece, high_piece, body, 0)

    cut = pieces // 2
    for t in range(half - 1):
        round_of(t, 0, cut)
    round_of(0, cut, pieces)
    round_of(half - 1, 0, cut)
    for t in range(1, half):
        round_of(t, cut, pieces)
        if t == 1:
            finish(0, cut)
    if half == 1:
        finish(0, cut)
    finish(cut, pieces)

    for c in range(dims["NC"]):
        at_piece, at_lane = c // (PIECE // 128), (c % (PIECE // 128)) * 128
        over_back[:, c, :] = over_total[at_piece, :, at_lane : at_lane + 128]
    over_ret[me_s] = over_back[me_s]
    for i in range(1, places):
        remote(
            over_back.at[place(i)], over_ret.at[me_s], over_send.at[1], over_recv.at[1], {"sp": place(i)}
        ).start()

    first = turned[:, 2:3]
    second = turned[:, 3:4]
    remote(
        over_back.at[0 : places - 1], over_ret.at[0 : places - 1], over_send.at[1], over_recv.at[1], right
    ).wait_recv()
    for c in range(dims["NC"]):
        at_piece, at_lane = c // (PIECE // 128), (c % (PIECE // 128)) * 128
        returned[at_piece, slots : slots + over, at_lane : at_lane + 128] = over_ret[:, c, :].astype(bf16)

    def combine(p, carry):
        remote(
            totals.at[p, 0 : (places - 1) * main, :],
            returned.at[p, 0 : (places - 1) * main, :],
            back_send.at[p],
            back_recv.at[p],
            right,
        ).wait_recv()
        span = pl.ds(pl.multiple_of(p * PIECE, PIECE), PIECE)
        one = jnp.dot(pick[0], returned[p], preferred_element_type=f32)
        two = jnp.dot(pick[1], returned[p], preferred_element_type=f32)
        out_ref[:, span] = (stream_ref[:, span].astype(f32) + (first * one + second * two)).astype(bf16)
        return carry

    lax.fori_loop(0, pieces, combine, 0)

    for n, (a, b) in enumerate(((over_out, over_in), (over_back, over_ret))):
        remote(
            a.at[0 : places - 1], b.at[0 : places - 1], over_send.at[n], over_recv.at[n], right
        ).wait_send()

    def drain(p, carry):
        span = pl.ds(0, (places - 1) * main)
        remote(
            outbound.at[p, span, :], chunks.at[me_x, p, span, :], out_send.at[p], out_recv.at[p], right
        ).wait_send()
        remote(
            totals.at[p, span, :], returned.at[p, span, :], back_send.at[p], back_recv.at[p], right
        ).wait_send()
        for way in range(2):
            for k in range(half):
                pl.when(k < far(way, p))(lambda way=way, k=k: ring(way, k, p, me_x).wait_send())
                pl.when(k < far(1 - way, p))(lambda way=way, k=k: hop(way, k + 1, p).wait_send())
        return carry

    lax.fori_loop(0, pieces, drain, 0)


def expert_layer(stream, gain, choice, share, gate_weight, up_weight, down_weight, places, columns):
    rows, width = stream.shape
    units = gate_weight.shape[2]
    f32, bf16 = jnp.float32, jnp.bfloat16
    main = 2 * rows // places
    over = -(-places // 16) * 16
    pieces, tiles, lanes = width // PIECE, units // 128, width // 128
    half = columns // 2
    total = places * main + over
    dims = dict(S=places, X=columns, R=rows, M=main, OV=over, NP=pieces, NT=tiles, NC=lanes)
    dma = pltpu.SemaphoreType.DMA
    whole = pl.BlockSpec(memory_space=pltpu.VMEM)
    away = pl.BlockSpec(memory_space=pl.ANY)
    return pl.pallas_call(
        functools.partial(expert_kernel, dims),
        out_shape=jax.ShapeDtypeStruct((rows, width), bf16),
        in_specs=[whole, whole, whole, whole, away, away, away],
        out_specs=whole,
        scratch_shapes=[
            pltpu.VMEM((8, rows), f32),
            pltpu.VMEM((pieces, places * main, PIECE), bf16),
            pltpu.VMEM((over, lanes, 128), f32),
            pltpu.VMEM((over, lanes, 128), f32),
            pltpu.VMEM((columns, pieces, total, PIECE), bf16),
            pltpu.VMEM((columns, total, units), bf16),
            pltpu.VMEM((tiles, width, 256), bf16),
            pltpu.VMEM((pieces, units, PIECE), bf16),
            pltpu.VMEM((half + 1, pieces, total, PIECE), bf16),
            pltpu.VMEM((half + 1, pieces, total, PIECE), bf16),
            pltpu.VMEM((pieces, places * main, PIECE), bf16),
            pltpu.VMEM((pieces, over, PIECE), f32),
            pltpu.VMEM((over, lanes, 128), f32),
            pltpu.VMEM((pieces, total, PIECE), bf16),
            pltpu.VMEM((over, lanes, 128), f32),
            pltpu.VMEM((2, rows, total), bf16),
            dma((2 * tiles + pieces,)),
            dma((pieces,)),
            dma((pieces,)),
            dma((2,)),
            dma((2,)),
            dma((2, half, pieces)),
            dma((2, half, pieces)),
            dma((2, half + 1, pieces)),
            dma((2, half + 1, pieces)),
            dma((pieces,)),
            dma((pieces,)),
        ],
        compiler_params=pltpu.CompilerParams(
            collective_id=0, has_side_effects=True, vmem_limit_bytes=VMEM_LIMIT
        ),
        name="routed_experts",
    )(stream, gain, choice, share, gate_weight, up_weight, down_weight)


def local(
    residual,
    grouped_value_heads,
    output_gate_heads,
    projected_key_query,
    raw_step_size,
    step_size_bias,
    head_decay_logarithm,
    position_extra_decay,
    head_skip_weight,
    value_kernel_taps,
    key_query_kernel,
    head_norm_gain,
    output_matrix,
    expert_norm_gain,
    expert_gate_weight,
    expert_up_weight,
    expert_down_weight,
    token_expert_choice,
    expert_output_weight,
):
    positions = grouped_value_heads.shape[0]
    lane_width = grouped_value_heads.shape[2]
    local_heads = lane_width // HEAD_DIM
    both_lanes = 2 * lane_width
    rim_depth = key_query_kernel.shape[0] - 1
    flat_values = grouped_value_heads.reshape(positions, both_lanes)
    rim_rows = jnp.concatenate(
        [flat_values[positions - rim_depth :], projected_key_query[positions - rim_depth :]], axis=1
    )
    prior_rows = passed_along(rim_rows, "sp", 1)
    padded_values = jnp.concatenate([prior_rows[:, :both_lanes], flat_values], axis=0)
    padded_keys = jnp.concatenate([prior_rows[:, both_lanes:], projected_key_query], axis=0)
    conv_heads = jax.nn.silu(
        causal_taps(padded_values, value_kernel_taps.reshape(rim_depth + 1, both_lanes), positions)
    ).astype(jnp.bfloat16)
    conv_rows = jax.nn.silu(causal_taps(padded_keys, key_query_kernel, positions)).astype(
        jnp.bfloat16
    )
    step_spacing = jax.nn.softplus(raw_step_size.astype(jnp.float32) + step_size_bias[None])
    decay_logarithm = (
        position_extra_decay[:, None, None] - jnp.exp(head_decay_logarithm)[None] * step_spacing
    )
    value_heads = conv_heads.reshape(positions, 2, local_heads, HEAD_DIM)
    bounds = [0, STATE_ONE, 2 * STATE_ONE, 2 * STATE_ONE + STATE_TWO, 2 * STATE_ONE + 2 * STATE_TWO]
    local_parts = []
    end_states = []
    decay_totals = []
    query_list = []
    reach_list = []
    for group_index in range(2):
        key_rows = conv_rows[:, bounds[2 * group_index] : bounds[2 * group_index + 1]]
        query_rows = conv_rows[:, bounds[2 * group_index + 1] : bounds[2 * group_index + 2]]
        local_part, end_state, decay_total, wide_queries, carried_decay = local_blocks(
            value_heads[:, group_index],
            key_rows,
            query_rows,
            step_spacing[:, group_index],
            decay_logarithm[:, group_index],
        )
        local_parts.append(local_part)
        end_states.append(end_state)
        decay_totals.append(decay_total)
        query_list.append(wide_queries)
        reach_list.append(carried_decay)
    identity = (
        jnp.zeros((2, local_heads), jnp.float32),
        jnp.zeros_like(end_states[0]),
        jnp.zeros_like(end_states[1]),
    )
    prior_decay, enter_one, enter_two = entering_2(
        (jnp.stack(decay_totals), end_states[0], end_states[1]), "sp", join_states, identity
    )
    entered = [enter_one, enter_two]
    group_parts = []
    for group_index in range(2):
        carried_part = jnp.einsum(
            "kln,hpn->klhp",
            query_list[group_index],
            entered[group_index],
            precision=lax.Precision.HIGHEST,
        )
        carried_part = carried_part * reach_list[group_index][:, :, :, None]
        summed_part = local_parts[group_index] + carried_part
        group_parts.append(summed_part.reshape(positions, local_heads, HEAD_DIM))
    mixer_sum = jnp.stack(group_parts, axis=1) + head_skip_weight[
        None, :, :, None
    ] * value_heads.astype(jnp.float32)
    gated_rows = mixer_sum * jax.nn.silu(
        output_gate_heads.astype(jnp.float32).reshape(positions, 2, local_heads, HEAD_DIM)
    )
    scale_rows = lax.rsqrt(jnp.mean(gated_rows * gated_rows, axis=3, keepdims=True) + EPSILON)
    mixed_heads = (
        gated_rows * scale_rows * head_norm_gain.reshape(2, local_heads, HEAD_DIM)
    ).astype(jnp.bfloat16)
    mixed_heads = mixed_heads.reshape(positions, 2, lane_width)
    rows_here = residual.shape[0]
    model_width = output_matrix.shape[2]
    moved = lax.all_to_all(mixed_heads, "tp", split_axis=0, concat_axis=2, tiled=True)
    mix_out = jnp.einsum(
        "tgc,gcd->td",
        moved,
        lax.all_gather(output_matrix, "tp", axis=1, tiled=True),
        preferred_element_type=jnp.float32,
    )
    stream = (residual.astype(jnp.float32) + mix_out).astype(jnp.bfloat16)
    return expert_layer(
        stream,
        expert_norm_gain[None],
        token_expert_choice.T,
        expert_output_weight.T,
        expert_gate_weight,
        expert_up_weight,
        expert_down_weight,
        lax.axis_size("sp"),
        lax.axis_size("tp"),
    )


def solution(mesh):
    placed = (
        P(("grp", "sp", "tp"), None),
        P(("grp", "sp"), None, "tp"),
        P(("grp", "sp"), None, "tp"),
        P(("grp", "sp"), None),
        P(("grp", "sp"), None, "tp"),
        P(None, "tp"),
        P(None, "tp"),
        P(("grp", "sp")),
        P(None, "tp"),
        P(None, None, "tp"),
        P(),
        P(None, "tp"),
        P(None, "tp", None),
        P(),
        P("sp", None, "tp"),
        P("sp", None, "tp"),
        P("sp", "tp", None),
        P(("grp", "sp", "tp"), None),
        P(("grp", "sp", "tp"), None),
    )
    return jax.shard_map(
        local, mesh=mesh, in_specs=placed, out_specs=P(("grp", "sp", "tp"), None), check_vma=False
    )
```

profile of v0, /device:TPU:513, one launch (start us, length us, event | category | flops | bytes accessed | tf_op | source)
XLA Modules:
  0.0 414.2 jit_solution(16598496117690356330)
XLA Ops:
  7.2 0.7 slice.211
  7.9 0.8 copy.212
  8.8 5.7 %collective-permute-start = (bf16[3,640]{0,1:T(8,128)(2,1)}, bf16[3,640]{0,1:T(8,128)(2,1)}, u32[]{:S(2)}, u32[]{:S(2)}) collective-permute-start(bf16[3,640]{0,1:T(8,128)(2,1)} %copy.212), channel_id=1, source_target_pairs={{0,8},{8,16},{16,24},{24,32},{32,40},{40,48},{48,56},{56,64},{64,7... | collective-permute-start | bytes 11528 | tf_op jit(solution)/shard_map/ppermute | solution.py:22
  15.3 0.8 multiply_subtract_fusion
  16.4 23.3 %fusion.58 = f32[8,128,2]{2,0,1:T(8,128)S(1)} fusion(f32[8,128,2]{2,0,1:T(8,128)S(1)} %copy.219), kind=kOutput, calls=%fused_computation.151 | output fusion | flops 260096 | bytes 16384 | tf_op jit(solution)/shard_map/jit(cumsum)/reduce_window_sum | solution.py:99
  40.1 23.3 %fusion.59 = f32[8,128,2]{2,0,1:T(8,128)S(1)} fusion(f32[8,128,2]{2,0,1:T(8,128)S(1)} %copy.233), kind=kOutput, calls=%fused_computation.152 | output fusion | flops 260096 | bytes 16384 | tf_op jit(solution)/shard_map/jit(cumsum)/reduce_window_sum | solution.py:99
  66.5 1.0 copy.236
  68.4 0.8 copy-done.3
  69.3 1.2 add_exponential_fusion
  71.0 2.0 copy.213
  73.0 0.8 copy.220
  73.8 0.8 copy.250
  74.6 0.8 copy.228
  76.1 1.8 copy.237
  78.7 0.8 copy.232
  79.7 0.8 copy.254
  81.9 0.8 slice.274
  82.8 1.0 multiply_convert_fusion.4
  83.8 0.8 fusion.57
  84.6 1.0 slice.280
  85.7 3.5 multiply_convert_fusion
  90.1 11.2 %while.26 = (s32[]{:T(128)}, f32[2,64,64]{2,1,0:T(8,128)S(1)}, f32[8,2,64,64]{3,2,1,0:T(8,128)}, f32[8,2]{1,0:T(8,128)}, f32[8,2,64,64]{3,2,1,0:T(8,128)S(1)}, /*index=5*/s32[]{:T(128)}, s32[]{:T(128)}) while((s32[]{:T(128)}, f32[2,64,64]{2,1,0:T(8,128)S(1)}, f32[8,2,64,64]{3,2,1,0:T(8,128)}, f32[8,2]{1,0:T(8,128)}, ...), condition=%wide.region_2.3_spmd.clone, body=%wide.region_1.2_spmd.clone.sunk | while | flops 32771 | bytes 197240 | solution.py:117
  90.8 0.7 fusion.78
  92.2 0.7 fusion.78
  93.6 0.7 fusion.78
  95.0 0.7 fusion.78
  96.4 0.7 fusion.78
  97.7 0.7 fusion.78
  99.1 0.7 fusion.78
  100.5 0.7 fusion.78
  101.4 1.0 copy.290
  103.1 11.2 %while.27 = (s32[]{:T(128)}, f32[2,64,128]{2,1,0:T(8,128)S(1)}, f32[8,2,64,128]{3,2,1,0:T(8,128)}, f32[8,2]{1,0:T(8,128)}, f32[8,2,64,128]{3,2,1,0:T(8,128)S(1)}, /*index=5*/s32[]{:T(128)}, s32[]{:T(128)}) while((s32[]{:T(128)}, f32[2,64,128]{2,1,0:T(8,128)S(1)}, f32[8,2,64,128]{3,2,1,0:T(8,128)}, f32[8,2]{1,0:T(8,128)}, ...), condition=%wide.region_5.6_spmd.clone, body=%wide.region_4.5_spmd.clone.sunk | while | flops 65539 | bytes 328312 | solution.py:117
  114.3 1.1 broadcast_in_dim.80
  115.4 20.2 %all-to-all-start = ((bf16[16,193,128]{2,1,0:T(8,128)(2,1)}), bf16[16,193,128]{2,1,0:T(8,128)(2,1)S(1)}, u32[]{:S(2)}, u32[]{:S(2)}) async-start(bf16[16,193,128]{2,1,0:T(8,128)(2,1)} %broadcast_in_dim.80), calls=%async_computation | async-start | bytes 1638400 | tf_op jit(solution)/shard_map/all_to_all | solution.py:27
  138.0 1.4 fusion.6
  139.4 1.3 fusion.7
  140.7 18.2 %all-to-all-done = bf16[16,193,128]{2,1,0:T(8,128)(2,1)S(1)} async-done(((bf16[16,193,128]{2,1,0:T(8,128)(2,1)}), bf16[16,193,128]{2,1,0:T(8,128)(2,1)S(1)}, u32[]{:S(2)}, u32[]{:S(2)}) %all-to-all-start) | async-done | bytes 790560 | tf_op jit(solution)/shard_map/all_to_all | solution.py:27
  159.7 0.9 slice_convert_fusion
  160.6 1.2 reshape.266
  162.8 0.7 copy-done.10
  164.3 0.9 stack_reshape.6
  166.1 0.7 copy-done.9
  167.6 0.9 stack_reshape.7
  168.6 1.6 fusion.14
  171.2 18.9 %all_to_all.23 = bf16[1024,2,128]{2,1,0:T(2,128)(2,1)S(1)} all-to-all(bf16[1024,2,128]{2,1,0:T(2,128)(2,1)S(1)} %copy.265), channel_id=1, replica_groups=mesh['grp'=2,'sp'=16,'tp'=8] {'tp'}, dimensions={0} | all-to-all | bytes 1048576 | tf_op jit(solution)/shard_map/all_to_all | solution.py:659
  190.7 5.4 %fusion.3.stream_ref = bf16[128,2048]{1,0:T(8,128)(2,1)} fusion(bf16[128,2,1024]{2,0,1:T(8,128)(2,1)S(1)} %all_to_all.20, bf16[2,1024,2048]{2,1,0:T(8,128)(2,1)} %all-gather.2.cloned.1.call-done, bf16[128,2048]{1,0:T(8,128)(2,1)S(1)} %copy-done.8), kind=kOutput, calls=%fused_computation.10 | convolution fusion | flops 1074528256 | bytes 9961472 | tf_op jit(solution)/shard_map/tgc,gcd->td/dot_general | solution.py:660
  196.1 209.3 %routed_experts.1 = bf16[128,2048]{1,0:T(8,128)(2,1)} custom-call(bf16[128,2048]{1,0:T(8,128)(2,1)} %fusion.3.stream_ref, f32[1,2048]{1,0:T(1,128)} %bitcast.235, s32[2,128]{1,0:T(2,128)} %bitcast.240, f32[2,128]{1,0:T(2,128)} %bitcast.241, bf16[1,2048,512]{2,1,0:T(8,128)(2,1)} %gate_hbm.1, bf16[1,2048,512]{2,1,0:T(8,128)(2,1)} %up_hbm.1, ...), custom_call_target="tpu_custom_call" | custom-call | tf_op jit(solution)/shard_map/routed_experts/pallas_call | solution.py:520
  405.5 1.9 copy.331
  (221 shorter events, 35.9 us)
Async XLA Ops:
  6.5 184.1 %all-gather.2.cloned.1.call-start = ((), (), s32[]{:S(2)}) async-start(), calls=%async_computation.2 | async-start | bytes 9437184 | tf_op jit(solution)/shard_map/all_gather | solution.py:663
  8.8 73.1 %collective-permute-start = (bf16[3,640]{0,1:T(8,128)(2,1)}, bf16[3,640]{0,1:T(8,128)(2,1)}, u32[]{:S(2)}, u32[]{:S(2)}) collective-permute-start(bf16[3,640]{0,1:T(8,128)(2,1)} %copy.212), channel_id=1, source_target_pairs={{0,8},{8,16},{16,24},{24,32},{32,40},{40,48},{48,56},{56,64},{64,7... | collective-permute-start | bytes 11528 | tf_op jit(solution)/shard_map/ppermute | solution.py:22
  16.4 48.7 %copy-start.36 = (bf16[4,2,128]{2,1,0:T(2,128)(2,1)S(1)}, bf16[4,2,128]{2,1,0:T(2,128)(2,1)}, u32[]{:S(2)}) copy-start(bf16[4,2,128]{2,1,0:T(2,128)(2,1)} %param.32) | copy-start | bytes 6148
  16.4 49.3 %copy-start.19 = (bf16[4,384]{1,0:T(4,128)(2,1)S(1)}, bf16[4,384]{1,0:T(4,128)(2,1)}, u32[]{:S(2)}) copy-start(bf16[4,384]{1,0:T(4,128)(2,1)} %param.33) | copy-start | bytes 9220
  68.2 1.0 copy-start.3
  73.8 5.9 %copy-start.2 = (f32[8,128,2]{2,0,1:T(8,128)S(1)}, f32[8,128,2]{2,0,1:T(8,128)}, u32[]{:S(2)}) copy-start(f32[8,128,2]{2,0,1:T(8,128)} %get-tuple-element.193) | copy-start | bytes 24580
  74.6 6.1 %copy-start.11 = (bf16[1024,2,128]{2,1,0:T(2,128)(2,1)S(1)}, bf16[1024,2,128]{2,1,0:T(2,128)(2,1)}, u32[]{:S(2)}) copy-start(bf16[1024,2,128]{2,1,0:T(2,128)(2,1)} %param.25) | copy-start | bytes 1572868
  78.6 2.6 copy-start.29
  78.6 4.1 copy-start.4
  78.6 4.1 copy-start.32
  78.6 4.1 copy-start.33
  78.6 4.1 copy-start.34
  78.7 4.1 copy-start.35
  81.3 4.4 %copy-start.22 = (f32[384]{0:T(512)S(1)}, f32[384]{0:T(512)}, u32[]{:S(2)}) copy-start(f32[384]{0:T(512)} %get-tuple-element.151) | copy-start | bytes 4612
  81.3 4.4 %copy-start.23 = (f32[384]{0:T(512)S(1)}, f32[384]{0:T(512)}, u32[]{:S(2)}) copy-start(f32[384]{0:T(512)} %get-tuple-element.152) | copy-start | bytes 4612
  81.3 4.4 %copy-start.24 = (f32[384]{0:T(512)S(1)}, f32[384]{0:T(512)}, u32[]{:S(2)}) copy-start(f32[384]{0:T(512)} %get-tuple-element.153) | copy-start | bytes 4612
  81.3 4.4 %copy-start.25 = (f32[384]{0:T(512)S(1)}, f32[384]{0:T(512)}, u32[]{:S(2)}) copy-start(f32[384]{0:T(512)} %get-tuple-element.154) | copy-start | bytes 4612
  84.6 5.0 %copy-start.6 = (bf16[16,8,8,128]{3,2,1,0:T(8,128)(2,1)}, bf16[16,8,8,128]{3,2,1,0:T(8,128)(2,1)S(1)}, u32[]{:S(2)}) copy-start(bf16[16,8,8,128]{3,2,1,0:T(8,128)(2,1)S(1)} %copy.286) | copy-start | bytes 786436
  85.7 3.9 copy-start.17
  89.4 0.7 copy-start
  101.3 1.2 copy-start.16
  102.5 11.8 %copy-start.38 = (bf16[1,128]{1,0:T(2,128)(2,1)S(1)}, bf16[1,128]{1,0:T(2,128)(2,1)}, u32[]{:S(2)}) copy-start(bf16[1,128]{1,0:T(2,128)(2,1)} %pad_bitcast_fusion) | copy-start | bytes 772
  114.2 21.3 %copy-start.1 = (bf16[1024,64]{1,0:T(8,128)(2,1)S(1)}, bf16[1024,64]{1,0:T(8,128)(2,1)}, u32[]{:S(2)}) copy-start(bf16[1024,64]{1,0:T(8,128)(2,1)} %copy-done) | copy-start | bytes 393220
  115.4 20.8 %copy-start.14 = (f32[8,128,2]{1,2,0:T(2,128)S(1)}, f32[8,128,2]{1,2,0:T(2,128)}, u32[]{:S(2)}) copy-start(f32[8,128,2]{1,2,0:T(2,128)} %copy.232) | copy-start | bytes 24580
  115.4 43.5 %all-to-all-start = ((bf16[16,193,128]{2,1,0:T(8,128)(2,1)}), bf16[16,193,128]{2,1,0:T(8,128)(2,1)S(1)}, u32[]{:S(2)}, u32[]{:S(2)}) async-start(bf16[16,193,128]{2,1,0:T(8,128)(2,1)} %broadcast_in_dim.80), calls=%async_computation | async-start | bytes 1638400 | tf_op jit(solution)/shard_map/all_to_all | solution.py:27
  135.6 1.0 copy-start.13
  135.6 1.7 copy-start.12
  135.6 1.7 copy-start.15
  136.2 1.8 copy-start.7
  136.2 1.8 copy-start.18
  136.2 1.8 copy-start.21
  136.2 1.8 copy-start.27
  137.3 2.1 copy-start.20
  137.3 2.1 copy-start.26
  139.4 19.6 %copy-start.28 = (pred[16]{0:T(512)(128)(4,1)S(1)}, pred[16]{0:T(512)(128)(4,1)}, u32[]{:S(2)}) copy-start(pred[16]{0:T(512)(128)(4,1)} %iota_compare_fusion.1) | copy-start | bytes 52
  162.5 1.0 copy-start.10
  165.8 1.0 copy-start.9
  167.3 1.3 copy-start.5
  167.3 1.3 copy-start.30
  168.5 1.7 copy-start.31
  168.5 1.7 copy-start.37
  171.1 19.5 %copy-start.8 = (bf16[128,2048]{1,0:T(8,128)(2,1)S(1)}, bf16[128,2048]{1,0:T(8,128)(2,1)}, u32[]{:S(2)}) copy-start(bf16[128,2048]{1,0:T(8,128)(2,1)} %param.23) | copy-start | bytes 1572868
Sparse Core Ops, SparseCore 0:
  14.7 110.9 all-gather.1
where the time goes:
time: 416 us; the launch traced here: 414 us
  Pallas kernels  209 us (50%)
  other arithmetic  71.2 us (17%)
  local copies, waits for them, and re-layouts  44.6 us (11%)
  starting transfers between devices  25.9 us (6%)
  blocking collectives  18.9 us (5%)
  waiting for transfers between devices  18.3 us (4%)
  between operations  14.2 us (3%)
  matrix products  11.7 us (3%)
    pallas_call x1, Pallas kernels, expert_layer(): pl.pallas_call(functools.partial(expert_kernel, dims), out_shape=jax.Shap...  209 us
    another operation x2, other arithmetic, local_blocks(): jnp.cumsum(decay_logarithm.reshape(block_count, BLOCK, head_count), axis=1)  46.6 us
    all_to_all x1, starting transfers between devices, sent_to_all(): lax.all_to_all(jnp.broadcast_to(shard[None], (length, *shard.shape)), axi...  20.2 us
    all_to_all x1, blocking collectives, local(): lax.all_to_all(mixed_heads, 'tp', split_axis=0, concat_axis=2, tiled=True)  18.9 us
    all_to_all x1, waiting for transfers between devices, sent_to_all(): lax.all_to_all(jnp.broadcast_to(shard[None], (length, *shard.shape)), axi...  18.2 us
    mul x16, local copies, waits for them, and re-layouts, advance(): return (carried * fading_step[:, None, None] + block_state, carried)  10.9 us
    unnamed x90, local copies, waits for them, and re-layouts  10.6 us
    dynamic_update_slice x16, other arithmetic, local_blocks(): lax.scan(advance, anchor, (states, jnp.exp(block_ends)))  10.1 us
  transfers between devices with their start and end apart: 3, of which 1 were waited for; matrix products, arithmetic and copies ran while one was open for 28% of the time, Pallas kernels for 0%

commit v1 on v0

--- a/solution.py
+++ b/solution.py
@@ -11,134 +11,7 @@
 STATE_ONE = 64
 STATE_TWO = 128
 BLOCK = 128
-
-
 EPSILON = 1e-06
-
-
-def passed_along(shard, axis, by):
-    length = lax.axis_size(axis)
-    pairs = [(i, i + by) for i in range(length) if 0 <= i + by < length]
-    return lax.ppermute(shard, axis, pairs)
-
-
-def sent_to_all(shard, axis):
-    length = lax.axis_size(axis)
-    return lax.all_to_all(
-        jnp.broadcast_to(shard[None], (length, *shard.shape)), axis, 0, 0, tiled=True
-    )
-
-
-def all_in_one(shard, axis):
-    leaves = jax.tree.leaves(shard)
-    turns = sorted(range(len(leaves)), key=lambda k: -leaves[k].size)
-    width = (1, *leaves[turns[0]].shape)[-1]
-    lines = [
-        jnp.pad(leaves[k].reshape(-1), (0, -leaves[k].size % width)).reshape(-1, width)
-        for k in turns
-    ]
-    both, at, found = (sent_to_all(jnp.concatenate(lines), axis), 0, {})
-    for k, line in zip(turns, lines):
-        section = both[:, at : at + len(line)].reshape(len(both), -1)
-        found[k] = section[:, : leaves[k].size].reshape(-1, *leaves[k].shape)
-        at += len(line)
-    numbers = iter(range(len(leaves)))
-    return jax.tree.map(lambda _: found[next(numbers)], shard)
-
-
-def joined_by_halves(pieces, combine):
-    while len(jax.tree.leaves(pieces)[0]) > 1:
-        pieces = jax.vmap(combine)(
-            *(jax.tree.map(lambda part: part[side::2], pieces) for side in (0, 1))
-        )
-    return jax.tree.map(lambda part: part[0], pieces)
-
-
-def entering_2(shard, axis, combine, identity):
-    length, place = (lax.axis_size(axis), lax.axis_index(axis))
-    passed = jnp.arange(length) < place
-
-    def kept(part, zero, own):
-        part = jnp.where(
-            passed.reshape(-1, *(1 for _ in own.shape)),
-            part.astype(own.dtype),
-            jnp.asarray(zero, own.dtype),
-        )
-        return part
-
-    pieces = all_in_one(
-        jax.tree.map(
-            lambda part, kind: part.astype(kind), shard, (jnp.bfloat16, jnp.bfloat16, jnp.bfloat16)
-        ),
-        axis,
-    )
-    return joined_by_halves(jax.tree.map(kept, pieces, identity, shard), combine)
-
-
-def causal_taps(extended, tap_weights, length):
-    summed = jnp.zeros((length, extended.shape[1]), jnp.float32)
-    for offset in range(tap_weights.shape[0]):
-        summed = summed + extended[offset : offset + length].astype(jnp.float32) * tap_weights[
-            offset
-        ].astype(jnp.float32)
-    return summed
-
-
-def advance(carried, pair_item):
-    block_state, fading_step = pair_item
-    return (carried * fading_step[:, None, None] + block_state, carried)
-
-
-def local_blocks(value_rows, key_rows, query_rows, step_spacing, decay_logarithm):
-    positions, head_count, head_width = value_rows.shape
-    block_count = positions // BLOCK
-    value_rows = value_rows.reshape(block_count, BLOCK, head_count, head_width)
-    key_rows = key_rows.reshape(block_count, BLOCK, key_rows.shape[-1])
-    query_rows = query_rows.reshape(block_count, BLOCK, query_rows.shape[-1])
-    step_spacing = step_spacing.reshape(block_count, BLOCK, head_count)
-    running = jnp.cumsum(decay_logarithm.reshape(block_count, BLOCK, head_count), axis=1)
-    scores = jnp.einsum("kln,ksn->kls", query_rows, key_rows, preferred_element_type=jnp.float32)
-    causal = jnp.tril(jnp.ones((BLOCK, BLOCK), jnp.bool_))
-    spread = running[:, :, None, :] - running[:, None, :, :]
-    damping = jnp.exp(jnp.where(causal[None, :, :, None], spread, -jnp.inf))
-    weights = (scores[:, :, :, None] * damping * step_spacing[:, None, :, :]).astype(jnp.bfloat16)
-    near_part = jnp.einsum(
-        "klsh,kshp->klhp", weights, value_rows, preferred_element_type=jnp.float32
-    )
-    fading = jnp.exp(running[:, -1:, :] - running) * step_spacing
-    scaled_keys = (key_rows.astype(jnp.float32)[:, :, None, :] * fading[:, :, :, None]).astype(
-        jnp.bfloat16
-    )
-    states = jnp.einsum(
-        "kshn,kshp->khpn", scaled_keys, value_rows, preferred_element_type=jnp.float32
-    )
-    block_ends = running[:, -1, :]
-    anchor = jnp.zeros(states.shape[1:], jnp.float32)
-    last_state, entering = lax.scan(advance, anchor, (states, jnp.exp(block_ends)))
-    wide_queries = query_rows.astype(jnp.float32)
-    far_part = jnp.einsum("kln,khpn->klhp", wide_queries, entering, precision=lax.Precision.HIGHEST)
-    far_part = far_part * jnp.exp(running)[:, :, :, None]
-    earlier_ends = jnp.cumsum(block_ends, axis=0) - block_ends
-    carried_decay = jnp.exp(running + earlier_ends[:, None, :])
-    return (
-        near_part + far_part,
-        last_state,
-        jnp.sum(block_ends, axis=0),
-        wide_queries,
-        carried_decay,
-    )
-
-
-def join_states(earlier, later):
-    early_decay, early_one, early_two = earlier
-    late_decay, late_one, late_two = later
-    return (
-        early_decay + late_decay,
-        early_one * jnp.exp(late_decay[0])[:, None, None] + late_one,
-        early_two * jnp.exp(late_decay[1])[:, None, None] + late_two,
-    )
-
-
 MESH = pl.DeviceIdType.MESH
 PIECE = 256
 VMEM_LIMIT = 67043328
@@ -558,6 +431,514 @@
     )(stream, gain, choice, share, gate_weight, up_weight, down_weight)
 
 
+def mixer_kernel(
+    dims,
+    residual_ref,
+    value_hbm,
+    gate_hbm,
+    keys_hbm,
+    raw_ref,
+    bias_ref,
+    log_ref,
+    extra_ref,
+    skip_ref,
+    value_tap_ref,
+    key_tap_ref,
+    gain_ref,
+    matrix_hbm,
+    out_ref,
+    value_in,
+    gate_in,
+    keys_in,
+    value_rim,
+    keys_rim,
+    value_wide,
+    keys_wide,
+    gate_wide,
+    conv_wide,
+    x_s,
+    kt_s,
+    q_s,
+    state_s,
+    near_s,
+    stride_s,
+    run_s,
+    fade_s,
+    end_s,
+    cols_s,
+    own_pack,
+    own_fade,
+    mate_pack,
+    mate_fade,
+    chip_pack,
+    chip_fade,
+    all_pack,
+    all_fade,
+    enter_pack,
+    carry_s,
+    mixed_s,
+    heads_in,
+    matrix,
+    acc_s,
+    load_sem,
+    rim_send,
+    rim_recv,
+    mate_send,
+    mate_recv,
+    chip_send,
+    chip_recv,
+    enter_send,
+    enter_recv,
+    head_send,
+    head_recv,
+    ring_send,
+    ring_recv,
+    pass_send,
+    pass_recv,
+):
+    f32, bf16 = jnp.float32, jnp.bfloat16
+    places, columns, width = dims["S"], dims["X"], dims["D"]
+    blocks = columns
+    rows = BLOCK
+    half = columns // 2
+    chips = places // 2
+    me_x, me_s = lax.axis_index("tp"), lax.axis_index("sp")
+    core = lax.rem(me_s, 2)
+    me_y = lax.div(me_s, 2)
+    right = {"tp": lax.rem(me_x + 1, columns)}
+    left = {"tp": lax.rem(me_x + columns - 1, columns)}
+    mate = {"sp": me_s + 1 - 2 * core}
+    following = {"sp": lax.rem(me_s + 1, places)}
+    previous = {"sp": lax.rem(me_s + places - 1, places)}
+
+    def column(offset):
+        return lax.rem(me_x + offset + columns, columns)
+
+    def peer(offset):
+        return {"sp": lax.rem(me_s + 2 * offset, places)}
+
+    def remote(src, dst, send, recv, device):
+        return pltpu.make_async_remote_copy(
+            src_ref=src, dst_ref=dst, send_sem=send, recv_sem=recv, device_id=device, device_id_type=MESH
+        )
+
+    loads = [
+        (matrix_hbm.at[0], matrix.at[me_x, pl.ds(0, rows), :]),
+        (matrix_hbm.at[1], matrix.at[me_x, pl.ds(rows, rows), :]),
+        (value_hbm, value_in),
+        (keys_hbm, keys_in),
+        (gate_hbm, gate_in),
+    ]
+    loads = [pltpu.make_async_copy(a, b, load_sem.at[n]) for n, (a, b) in enumerate(loads)]
+    for load in loads:
+        load.start()
+
+    barrier = pltpu.get_barrier_semaphore()
+    peers = [{"tp": column(i)} for i in range(1, columns)]
+    peers += [peer(i) for i in range(1, chips)] + [following, previous]
+    for device in peers:
+        pl.semaphore_signal(barrier, inc=1, device_id=device, device_id_type=MESH)
+
+    heads = 4
+    for g in range(2):
+        raw = raw_ref[g].astype(f32)
+        for k in range(blocks):
+            stride_s[heads * k + 2 * g : heads * k + 2 * g + 2, :] = raw[:, k * rows : (k + 1) * rows]
+    for k in range(blocks):
+        run_s[heads * k : heads * k + heads, :] = jnp.broadcast_to(extra_ref[k : k + 1, :], (heads, rows))
+    head_of = jnp.bitwise_and(lax.broadcasted_iota(jnp.int32, (heads * blocks, rows), 0), heads - 1)
+
+    def by_head(table):
+        picked = jnp.full((heads * blocks, rows), table[1, 1], f32)
+        for n in range(3):
+            picked = jnp.where(head_of == n, table[n // 2, n % 2], picked)
+        return picked
+
+    shifted = stride_s[...] + by_head(bias_ref)
+    stride = jnp.maximum(shifted, 0.0) + jnp.log1p(jnp.exp(-jnp.abs(shifted)))
+    log_decay = run_s[...] - jnp.exp(by_head(log_ref)) * stride
+    at_row = lax.broadcasted_iota(jnp.int32, (rows, rows), 0)
+    at_lane = lax.broadcasted_iota(jnp.int32, (rows, rows), 1)
+    running = jnp.dot(
+        log_decay,
+        jnp.where(at_row <= at_lane, 1.0, 0.0),
+        preferred_element_type=f32,
+        precision=lax.Precision.HIGHEST,
+    )
+    ends = jnp.broadcast_to(running[:, rows - 1 : rows], running.shape)
+    stride_s[...] = stride
+    run_s[...] = running
+    fade_s[...] = jnp.exp(ends - running) * stride
+    end_s[...] = jnp.exp(ends)
+    turned = jnp.transpose(running)
+    for k in range(blocks):
+        cols_s[k, :, 0:heads] = turned[:, heads * k : heads * k + heads]
+
+    first_head = lax.broadcasted_iota(jnp.int32, (rows, rows), 1) < HEAD_DIM
+
+    def row_pair(table, k, g):
+        low = table[pl.ds(heads * k + 2 * g, 1), :]
+        high = table[pl.ds(heads * k + 2 * g + 1, 1), :]
+        return jnp.where(first_head[0:1], low, high)
+
+    pl.semaphore_wait(barrier, len(peers))
+    for load in loads[:4]:
+        load.wait()
+
+    cut = width // 2
+    mine = pl.ds(pl.multiple_of(core * rows, rows), rows)
+
+    def ring(way, event, col):
+        lanes = pl.ds(((event % 2) ^ way) * cut, cut)
+        here = matrix.at[col, mine, lanes]
+        return remote(
+            here, here, ring_send.at[way, event], ring_recv.at[way, event], right if way == 0 else left
+        )
+
+    def passing(way, event, col):
+        lanes = pl.ds(((event % 2) ^ way) * cut, cut)
+        here = matrix.at[col, mine, lanes]
+        return remote(here, here, pass_send.at[way, event], pass_recv.at[way, event], mate)
+
+    for event in range(2):
+        for way in range(2):
+            if event < columns - 1:
+                ring(way, event, me_x).start()
+
+    def service(event):
+        k = event // 2 + 1
+        for way in range(2):
+            col = column(-k if way == 0 else k)
+            ring(way, event, col).wait_recv()
+            if event + 2 < columns - 1:
+                ring(way, event + 2, col).start()
+            passing(way, event, col).start()
+
+    rim_rows = 16
+    positions = blocks * rows
+    rims = [
+        remote(
+            value_in.at[pl.ds(2 * positions - rim_rows, rim_rows), :], value_rim, rim_send.at[0], rim_recv.at[0], following
+        ),
+        remote(keys_in.at[pl.ds(positions - rim_rows, rim_rows), :], keys_rim, rim_send.at[1], rim_recv.at[1], following),
+    ]
+    for rim in rims:
+        rim.start()
+
+    def silu(a):
+        return a * (1.0 / (1.0 + jnp.exp(-a)))
+
+    value_wide[rim_rows:, :] = value_in[...].astype(f32)
+    keys_wide[rim_rows:, :] = keys_in[...].astype(f32)
+    taps = value_tap_ref.shape[0] // 2
+    value_tap = value_tap_ref[...].astype(f32)
+    key_tap = key_tap_ref[...].astype(f32)
+    even = jnp.bitwise_and(lax.broadcasted_iota(jnp.int32, (2 * rows, rows), 0), 1) == 0
+    tap_rows = [jnp.where(even, value_tap[2 * j : 2 * j + 1], value_tap[2 * j + 1 : 2 * j + 2]) for j in range(taps)]
+
+    def states_of(k):
+        base = pl.multiple_of(k * 2 * rows, 2 * rows)
+        window = value_wide[pl.ds(base, 2 * rows + rim_rows), :]
+        total = jnp.zeros((2 * rows, rows), f32)
+        for j in range(taps):
+            start = rim_rows - 2 * (taps - 1 - j)
+            total = total + window[start : start + 2 * rows] * tap_rows[j]
+        conv_wide[...] = silu(total).astype(bf16).astype(f32)
+        low = pl.multiple_of(k * rows, rows)
+        window = keys_wide[pl.ds(low, rows + rim_rows), :]
+        total = jnp.zeros((rows, keys_wide.shape[1]), f32)
+        for j in range(taps):
+            start = rim_rows - (taps - 1 - j)
+            total = total + window[start : start + rows] * key_tap[j : j + 1]
+        conv = silu(total).astype(bf16).astype(f32)
+        both = conv[:, 0 : 2 * STATE_ONE]
+        keys = [jnp.where(first_head, both, 0.0), conv[:, 2 * STATE_ONE : 2 * STATE_ONE + STATE_TWO]]
+        asks = [pltpu.roll(both, STATE_ONE, 1), conv[:, 2 * STATE_ONE + STATE_TWO :]]
+        for g in range(2):
+            x = conv_wide[pl.ds(g, rows, stride=2), :].astype(bf16)
+            key_t = jnp.transpose(keys[g])
+            x_s[k, g] = x
+            kt_s[k, g] = key_t.astype(bf16)
+            q_s[k, g] = asks[g].astype(bf16)
+            faded = jnp.concatenate(
+                [key_t * fade_s[pl.ds(heads * k + 2 * g + h, 1), :] for h in range(2)], axis=0
+            ).astype(bf16)
+            state = jnp.dot(faded, x, preferred_element_type=f32)
+            state_s[k, g] = jnp.where(first_head, state[:rows], state[rows:])
+
+    def state_step(i, carry):
+        states_of(i)
+        return carry
+
+    lax.fori_loop(1, blocks, state_step, 0)
+    for rim in rims:
+        rim.wait_recv()
+    opening = me_s == 0
+    value_wide[0:rim_rows, :] = jnp.where(opening, 0.0, value_rim[...].astype(f32))
+    keys_wide[0:rim_rows, :] = jnp.where(opening, 0.0, keys_rim[...].astype(f32))
+    states_of(0)
+
+    packed = STATE_TWO + STATE_ONE
+    piece = packed // 2
+
+    def local_end(g):
+        total = jnp.zeros((rows, rows), f32)
+        faded = jnp.ones((1, rows), f32)
+        for k in range(blocks):
+            decay = row_pair(end_s, k, g)
+            total = total * decay + state_s[k, g]
+            faded = faded * decay
+        return total, faded
+
+    end_one, fade_one = local_end(0)
+    end_two, fade_two = local_end(1)
+    own = jnp.concatenate([end_two, end_one[:STATE_ONE]], axis=0)
+    own_pack[...] = own.astype(bf16)
+    own_fade[0:1, :] = fade_one
+    own_fade[1:2, :] = fade_two
+    own_fade[2:8, :] = jnp.zeros((6, rows), f32)
+    mates = [
+        remote(own_pack, mate_pack, mate_send.at[0], mate_recv.at[0], mate),
+        remote(own_fade, mate_fade, mate_send.at[1], mate_recv.at[1], mate),
+    ]
+    for copy in mates:
+        copy.start()
+    service(0)
+    for copy in mates:
+        copy.wait_recv()
+    is_low = core == 0
+    low = jnp.where(is_low, own, mate_pack[...].astype(f32))
+    high = jnp.where(is_low, mate_pack[...].astype(f32), own)
+    mate_rows = mate_fade[...]
+    own_rows = own_fade[...]
+    high_rows = jnp.where(is_low, mate_rows, own_rows)
+    in_two = lax.broadcasted_iota(jnp.int32, (packed, rows), 0) < STATE_TWO
+    chip_pack[...] = (low * jnp.where(in_two, high_rows[1:2], high_rows[0:1]) + high).astype(bf16)
+    chip_fade[...] = own_rows * mate_rows
+    my_half = pl.ds(pl.multiple_of(core * piece, 16), piece)
+
+    def to_chip(n, which):
+        src = chip_pack.at[my_half, :] if which == 0 else chip_fade
+        dst = all_pack.at[me_y] if which == 0 else all_fade.at[me_y]
+        return remote(src, dst, chip_send.at[which, n], chip_recv.at[which, n], peer(n))
+
+    for n in range(1, chips):
+        for which in range(2):
+            to_chip(n, which).start()
+
+    below = at_row >= at_lane
+
+    def near_step(k, carry):
+        cols = cols_s[k]
+        for g in range(2):
+            scores = jnp.dot(q_s[k, g], kt_s[k, g], preferred_element_type=f32)
+            parts = []
+            for h in range(2):
+                n = 2 * g + h
+                gap = cols[:, n : n + 1] - run_s[pl.ds(heads * k + n, 1), :]
+                damping = jnp.exp(jnp.where(below, gap, -1e30))
+                parts.append((scores * damping * stride_s[pl.ds(heads * k + n, 1), :]).astype(bf16))
+            near = jnp.dot(jnp.concatenate(parts, axis=0), x_s[k, g], preferred_element_type=f32)
+            near_s[k, g] = jnp.where(first_head, near[:rows], near[rows:])
+        return carry
+
+    lax.fori_loop(0, blocks, near_step, 0)
+    if columns > 2:
+        service(1)
+    loads[4].wait()
+
+    for n in range(1, chips):
+        for which in range(2):
+            to_chip(n, which).wait_recv()
+    row_at = lax.broadcasted_iota(jnp.int32, (piece, rows), 0) + core * piece
+    half_two = row_at < STATE_TWO
+    entering = jnp.zeros((piece, rows), f32)
+    for y in range(chips):
+        fades = all_fade[y]
+        later = entering * jnp.where(half_two, fades[1:2], fades[0:1]) + all_pack[y].astype(f32)
+        entering = jnp.where(y < me_y, later, entering)
+    enter_pack[my_half, :] = entering.astype(bf16)
+    here = enter_pack.at[my_half, :]
+    enter_copy = remote(here, here, enter_send.at[0], enter_recv.at[0], mate)
+    enter_copy.start()
+    enter_copy.wait_recv()
+    chip_state = enter_pack[...].astype(f32)
+    after_low = chip_state * jnp.where(in_two, mate_rows[1:2], mate_rows[0:1]) + mate_pack[...].astype(f32)
+    entered = jnp.where(is_low, chip_state, after_low)
+    carry_s[1] = entered[:STATE_TWO]
+    carry_s[0] = jnp.zeros((rows, rows), f32)
+    carry_s[0, 0:STATE_ONE, :] = entered[STATE_TWO:]
+
+    def head_copy(col):
+        return remote(mixed_s.at[col], heads_in.at[me_x], head_send.at[col], head_recv.at[me_x], {"tp": col})
+
+    def mix_step(k, carry):
+        cols = jnp.exp(cols_s[k])
+        gate_wide[...] = gate_in[pl.ds(pl.multiple_of(k * 2 * rows, 2 * rows), 2 * rows), :].astype(f32)
+        for g in range(2):
+            state = carry_s[g]
+            coarse = state.astype(bf16)
+            fine = (state - coarse.astype(f32)).astype(bf16)
+            ask = q_s[k, g]
+            far = jnp.dot(
+                jnp.concatenate([ask, ask], axis=1),
+                jnp.concatenate([coarse, fine], axis=0),
+                preferred_element_type=f32,
+            )
+            reach = jnp.where(first_head, cols[:, 2 * g : 2 * g + 1], cols[:, 2 * g + 1 : 2 * g + 2])
+            skip = jnp.where(first_head[0:1], skip_ref[g, 0], skip_ref[g, 1])
+            mixed = near_s[k, g] + far * reach + skip * x_s[k, g].astype(f32)
+            gate = gate_wide[pl.ds(g, rows, stride=2), :]
+            gated = mixed * silu(gate)
+            square = gated * gated
+            one = jnp.sum(jnp.where(first_head, square, 0.0), axis=1, keepdims=True)
+            two = jnp.sum(jnp.where(first_head, 0.0, square), axis=1, keepdims=True)
+            scale = lax.rsqrt(jnp.where(first_head, one, two) * (1.0 / HEAD_DIM) + EPSILON)
+            mixed_s[k, :, g * rows : (g + 1) * rows] = (gated * scale * gain_ref[g : g + 1, :]).astype(bf16)
+            carry_s[g] = state * row_pair(end_s, k, g) + state_s[k, g]
+
+        @pl.when(k != me_x)
+        def _():
+            head_copy(k).start()
+
+        return carry
+
+    lax.fori_loop(0, blocks, mix_step, 0)
+    heads_in[me_x] = mixed_s[me_x]
+
+    def arrived(col):
+        return remote(mixed_s.at[col], heads_in.at[col], head_send.at[col], head_recv.at[col], {"tp": col})
+
+    def product(col, first=False):
+        for n in range(0, width, 512):
+            part = jnp.dot(heads_in[col], matrix[col, :, n : n + 512], preferred_element_type=f32)
+            acc_s[:, n : n + 512] = part if first else acc_s[:, n : n + 512] + part
+
+    product(me_x, True)
+    for event in range(2, columns - 1):
+        service(event)
+    for k in range(1, half + 1):
+        for way in range(2):
+            if way == 1 and k == half:
+                continue
+            for event in (2 * k - 2, 2 * k - 1):
+                if event < columns - 1:
+                    if k == half:
+                        for side in range(2):
+                            passing(side, event, column(k)).wait_recv()
+                    else:
+                        passing(way, event, column(k)).wait_recv()
+            col = column(-k if way == 0 else k)
+            arrived(col).wait_recv()
+            product(col)
+    out_ref[...] = (residual_ref[...].astype(f32) + acc_s[...]).astype(bf16)
+
+    for copy in rims + mates + [enter_copy]:
+        copy.wait_send()
+    for n in range(1, chips):
+        for which in range(2):
+            to_chip(n, which).wait_send()
+    for i in range(1, columns):
+        head_copy(column(i)).wait_send()
+    for event in range(columns - 1):
+        for way in range(2):
+            ring(way, event, me_x).wait_send()
+            passing(way, event, me_x).wait_send()
+
+
+def mixer_layer(
+    residual, values, gates, keys, raw, bias, logarithm, extra, skip, value_taps, key_taps, gain, matrix, places, columns
+):
+    f32, bf16 = jnp.float32, jnp.bfloat16
+    rows, width = residual.shape
+    positions = values.shape[0]
+    lanes = keys.shape[1]
+    blocks = positions // BLOCK
+    chips = places // 2
+    packed = STATE_ONE + STATE_TWO
+    dma = pltpu.SemaphoreType.DMA
+    whole = pl.BlockSpec(memory_space=pltpu.VMEM)
+    away = pl.BlockSpec(memory_space=pl.ANY)
+    scalars = pl.BlockSpec(memory_space=pltpu.SMEM)
+    square = (blocks, 2, BLOCK, BLOCK)
+    return pl.pallas_call(
+        functools.partial(mixer_kernel, dict(S=places, X=columns, D=width)),
+        out_shape=jax.ShapeDtypeStruct((rows, width), bf16),
+        in_specs=[
+            whole, away, away, away, whole, scalars, scalars, whole, scalars, whole, whole, whole, away,
+        ],
+        out_specs=whole,
+        scratch_shapes=[
+            pltpu.VMEM((2 * positions, BLOCK), bf16),
+            pltpu.VMEM((2 * positions, BLOCK), bf16),
+            pltpu.VMEM((positions, lanes), bf16),
+            pltpu.VMEM((16, BLOCK), bf16),
+            pltpu.VMEM((16, lanes), bf16),
+            pltpu.VMEM((2 * positions + 16, BLOCK), f32),
+            pltpu.VMEM((positions + 16, lanes), f32),
+            pltpu.VMEM((2 * BLOCK, BLOCK), f32),
+            pltpu.VMEM((2 * BLOCK, BLOCK), f32),
+            pltpu.VMEM(square, bf16),
+            pltpu.VMEM(square, bf16),
+            pltpu.VMEM(square, bf16),
+            pltpu.VMEM(square, f32),
+            pltpu.VMEM(square, f32),
+            pltpu.VMEM((4 * blocks, BLOCK), f32),
+            pltpu.VMEM((4 * blocks, BLOCK), f32),
+            pltpu.VMEM((4 * blocks, BLOCK), f32),
+            pltpu.VMEM((4 * blocks, BLOCK), f32),
+            pltpu.VMEM((blocks, BLOCK, 4), f32),
+            pltpu.VMEM((packed, BLOCK), bf16),
+            pltpu.VMEM((8, BLOCK), f32),
+            pltpu.VMEM((packed, BLOCK), bf16),
+            pltpu.VMEM((8, BLOCK), f32),
+            pltpu.VMEM((packed, BLOCK), bf16),
+            pltpu.VMEM((8, BLOCK), f32),
+            pltpu.VMEM((chips, packed // 2, BLOCK), bf16),
+            pltpu.VMEM((chips, 8, BLOCK), f32),
+            pltpu.VMEM((packed, BLOCK), bf16),
+            pltpu.VMEM((2, BLOCK, BLOCK), f32),
+            pltpu.VMEM((columns, BLOCK, 2 * BLOCK), bf16),
+            pltpu.VMEM((columns, BLOCK, 2 * BLOCK), bf16),
+            pltpu.VMEM((columns, 2 * BLOCK, width), bf16),
+            pltpu.VMEM((rows, width), f32),
+            dma((5,)),
+            dma((2,)),
+            dma((2,)),
+            dma((2,)),
+            dma((2,)),
+            dma((2, chips)),
+            dma((2, chips)),
+            dma((1,)),
+            dma((1,)),
+            dma((columns,)),
+            dma((columns,)),
+            dma((2, columns - 1)),
+            dma((2, columns - 1)),
+            dma((2, columns - 1)),
+            dma((2, columns - 1)),
+        ],
+        compiler_params=pltpu.CompilerParams(
+            collective_id=1, has_side_effects=True, vmem_limit_bytes=VMEM_LIMIT
+        ),
+        name="mixer",
+    )(
+        residual,
+        values.reshape(2 * positions, BLOCK),
+        gates.reshape(2 * positions, BLOCK),
+        keys,
+        raw.transpose(1, 2, 0),
+        bias,
+        logarithm,
+        extra.reshape(blocks, BLOCK),
+        skip,
+        value_taps.reshape(-1, BLOCK),
+        key_taps,
+        gain,
+        matrix,
+    )
+
+
 def local(
     residual,
     grouped_value_heads,
@@ -579,91 +960,24 @@
     token_expert_choice,
     expert_output_weight,
 ):
-    positions = grouped_value_heads.shape[0]
-    lane_width = grouped_value_heads.shape[2]
-    local_heads = lane_width // HEAD_DIM
-    both_lanes = 2 * lane_width
-    rim_depth = key_query_kernel.shape[0] - 1
-    flat_values = grouped_value_heads.reshape(positions, both_lanes)
-    rim_rows = jnp.concatenate(
-        [flat_values[positions - rim_depth :], projected_key_query[positions - rim_depth :]], axis=1
+    places, columns = lax.axis_size("sp"), lax.axis_size("tp")
+    stream = mixer_layer(
+        residual,
+        grouped_value_heads,
+        output_gate_heads,
+        projected_key_query,
+        raw_step_size,
+        step_size_bias,
+        head_decay_logarithm,
+        position_extra_decay,
+        head_skip_weight,
+        value_kernel_taps,
+        key_query_kernel,
+        head_norm_gain,
+        output_matrix,
+        places,
+        columns,
     )
-    prior_rows = passed_along(rim_rows, "sp", 1)
-    padded_values = jnp.concatenate([prior_rows[:, :both_lanes], flat_values], axis=0)
-    padded_keys = jnp.concatenate([prior_rows[:, both_lanes:], projected_key_query], axis=0)
-    conv_heads = jax.nn.silu(
-        causal_taps(padded_values, value_kernel_taps.reshape(rim_depth + 1, both_lanes), positions)
-    ).astype(jnp.bfloat16)
-    conv_rows = jax.nn.silu(causal_taps(padded_keys, key_query_kernel, positions)).astype(
-        jnp.bfloat16
-    )
-    step_spacing = jax.nn.softplus(raw_step_size.astype(jnp.float32) + step_size_bias[None])
-    decay_logarithm = (
-        position_extra_decay[:, None, None] - jnp.exp(head_decay_logarithm)[None] * step_spacing
-    )
-    value_heads = conv_heads.reshape(positions, 2, local_heads, HEAD_DIM)
-    bounds = [0, STATE_ONE, 2 * STATE_ONE, 2 * STATE_ONE + STATE_TWO, 2 * STATE_ONE + 2 * STATE_TWO]
-    local_parts = []
-    end_states = []
-    decay_totals = []
-    query_list = []
-    reach_list = []
-    for group_index in range(2):
-        key_rows = conv_rows[:, bounds[2 * group_index] : bounds[2 * group_index + 1]]
-        query_rows = conv_rows[:, bounds[2 * group_index + 1] : bounds[2 * group_index + 2]]
-        local_part, end_state, decay_total, wide_queries, carried_decay = local_blocks(
-            value_heads[:, group_index],
-            key_rows,
-            query_rows,
-            step_spacing[:, group_index],
-            decay_logarithm[:, group_index],
-        )
-        local_parts.append(local_part)
-        end_states.append(end_state)
-        decay_totals.append(decay_total)
-        query_list.append(wide_queries)
-        reach_list.append(carried_decay)
-    identity = (
-        jnp.zeros((2, local_heads), jnp.float32),
-        jnp.zeros_like(end_states[0]),
-        jnp.zeros_like(end_states[1]),
-    )
-    prior_decay, enter_one, enter_two = entering_2(
-        (jnp.stack(decay_totals), end_states[0], end_states[1]), "sp", join_states, identity
-    )
-    entered = [enter_one, enter_two]
-    group_parts = []
-    for group_index in range(2):
-        carried_part = jnp.einsum(
-            "kln,hpn->klhp",
-            query_list[group_index],
-            entered[group_index],
-            precision=lax.Precision.HIGHEST,
-        )
-        carried_part = carried_part * reach_list[group_index][:, :, :, None]
-        summed_part = local_parts[group_index] + carried_part
-        group_parts.append(summed_part.reshape(positions, local_heads, HEAD_DIM))
-    mixer_sum = jnp.stack(group_parts, axis=1) + head_skip_weight[
-        None, :, :, None
-    ] * value_heads.astype(jnp.float32)
-    gated_rows = mixer_sum * jax.nn.silu(
-        output_gate_heads.astype(jnp.float32).reshape(positions, 2, local_heads, HEAD_DIM)
-    )
-    scale_rows = lax.rsqrt(jnp.mean(gated_rows * gated_rows, axis=3, keepdims=True) + EPSILON)
-    mixed_heads = (
-        gated_rows * scale_rows * head_norm_gain.reshape(2, local_heads, HEAD_DIM)
-    ).astype(jnp.bfloat16)
-    mixed_heads = mixed_heads.reshape(positions, 2, lane_width)
-    rows_here = residual.shape[0]
-    model_width = output_matrix.shape[2]
-    moved = lax.all_to_all(mixed_heads, "tp", split_axis=0, concat_axis=2, tiled=True)
-    mix_out = jnp.einsum(
-        "tgc,gcd->td",
-        moved,
-        lax.all_gather(output_matrix, "tp", axis=1, tiled=True),
-        preferred_element_type=jnp.float32,
-    )
-    stream = (residual.astype(jnp.float32) + mix_out).astype(jnp.bfloat16)
     return expert_layer(
         stream,
         expert_norm_gain[None],
@@ -672,8 +986,8 @@
         expert_gate_weight,
         expert_up_weight,
         expert_down_weight,
-        lax.axis_size("sp"),
-        lax.axis_size("tp"),
+        places,
+        columns,
     )
 
 

time: 416 us -> 287 us (0.69)
  Pallas kernels: 209 us -> 284 us
  other arithmetic: 71.2 us -> 0 us
  local copies, waits for them, and re-layouts: 44.6 us -> 1.88 us
  starting transfers between devices: 25.9 us -> 0 us
  blocking collectives: 18.9 us -> 0 us
  waiting for transfers between devices: 18.3 us -> 0 us
  between operations: 14.2 us -> 0.02 us
  matrix products: 11.7 us -> 0 us
    pallas_call x0 -> x1, Pallas kernels: none -> 75.1 us  [mixer_layer(): pl.pallas_call(functools.partial(mixer_kernel, dict(S=places, X=columns,...]
    another operation x5 -> x0, other arithmetic: 46.7 us -> none  [the longest x2 46.6 us: local_blocks(): jnp.cumsum(decay_logarithm.reshape(block_count, BLOCK, head_count), axis=1)]
    all_to_all x1 -> x0, starting transfers between devices: 20.2 us -> none  [sent_to_all(): lax.all_to_all(jnp.broadcast_to(shard[None], (length, *shard.shape)), axi...]
    all_to_all x1 -> x0, blocking collectives: 18.9 us -> none  [local(): lax.all_to_all(mixed_heads, 'tp', split_axis=0, concat_axis=2, tiled=True)]
    all_to_all x1 -> x0, waiting for transfers between devices: 18.2 us -> none  [sent_to_all(): lax.all_to_all(jnp.broadcast_to(shard[None], (length, *shard.shape)), axi...]
    mul x22 -> x0, local copies, waits for them, and re-layouts: 15.1 us -> none  [the longest x16 10.9 us: advance(): return (carried * fading_step[:, None, None] + block_state, carried)]
    dot_general x11 -> x0, matrix products: 11.7 us -> none  [the longest x1 5.44 us: local(): jnp.einsum('tgc,gcd->td', moved, lax.all_gather(output_matrix, 'tp', axis...]
    dynamic_update_slice x16 -> x0, other arithmetic: 10.1 us -> none  [local_blocks(): lax.scan(advance, anchor, (states, jnp.exp(block_ends)))]
  transfers between devices with their start and end apart: 3 -> 0, of which waited for: 1 -> 0; matrix products, arithmetic and copies ran while one was open for 28% -> 0% of each run, Pallas kernels for 0% -> 0%
where the time goes in v1:
time: 287 us; the launch traced here: 286 us
  Pallas kernels  284 us (99%)
    pallas_call x1, Pallas kernels, expert_layer(): pl.pallas_call(functools.partial(expert_kernel, dims), out_shape=jax.Shap...  209 us
    pallas_call x1, Pallas kernels, mixer_layer(): pl.pallas_call(functools.partial(mixer_kernel, dict(S=places, X=columns,...  75.1 us

profile of v1, /device:TPU:513, one launch (start us, length us, event | category | flops | bytes accessed | tf_op | source)
XLA Modules:
  0.0 286.2 jit_solution(12596743769533099505)
XLA Ops:
  0.0 75.1 %mixer.1.stream_ref = bf16[128,2048]{1,0:T(8,128)(2,1)} custom-call(bf16[128,2048]{1,0:T(8,128)(2,1)} %residual_ref.1, bf16[2048,128]{1,0:T(8,128)(2,1)} %bitcast.8, bf16[2048,128]{1,0:T(8,128)(2,1)} %bitcast.9, bf16[1024,384]{1,0:T(8,128)(2,1)} %keys_hbm.1, bf16[2,2,1024]{2,1,0:T(2,128)(2,1)} %bitcast.10, f32[2,2]{1,0:T(2,128)} %bias_ref.1, ...), custom_call_target="tpu_custom_call" | custom-call | tf_op jit(solution)/shard_map/mixer/pallas_call | solution.py:864
  75.1 209.2 %routed_experts.1 = bf16[128,2048]{1,0:T(8,128)(2,1)} custom-call(bf16[128,2048]{1,0:T(8,128)(2,1)} %mixer.1.stream_ref, f32[1,2048]{1,0:T(1,128)} %bitcast.11, s32[2,128]{1,0:T(2,128)} %bitcast.14, f32[2,128]{1,0:T(2,128)} %bitcast.15, bf16[1,2048,512]{2,1,0:T(8,128)(2,1)} %gate_hbm.1, bf16[1,2048,512]{2,1,0:T(8,128)(2,1)} %up_hbm.1, ...), custom_call_target="tpu_custom_call" | custom-call | tf_op jit(solution)/shard_map/routed_experts/pallas_call | solution.py:393
  284.3 1.9 copy.21
